TPU v7x, 32 devices: a whole 2x2x4 slice. The times are simulated.
32 devices in a mesh: sp: 8 (over z, x), tp: 4 (over y, core).
Axes of the slice: x: 2, y: 2, z: 4, core: 2. Of those that a mesh axis runs over, the one named last changes fastest.
Arguments:
- stream_in: bfloat16 [2048, 2048], P(('sp', 'tp')), may hold values from -6 to 6
- pre_gate: bfloat16 [2048, 1024], P('sp', 'tp'), may hold values from -6 to 6
- value_in: bfloat16 [2048, 1024], P('sp', 'tp'), may hold values from -6 to 6
- post_gate: bfloat16 [2048, 1024], P('sp', 'tp'), may hold values from -6 to 6
- conv_taps: bfloat16 [3, 1024], P(None, 'tp'), may hold values from -3 to 3
- out_weight: bfloat16 [1024, 2048], P('tp'), may hold values from -0.1875 to 0.1875
- route_ids: int32 [2048, 4], P('sp'), may hold values from 0 to 7, all different within a row; in each aligned block of 64 rows (0 to 63, 64 to 127, ...) at most 64 rows name the same one
- route_weight: float32 [2048, 4], P('sp'), may hold values from 0.1 to 1
- ffn_gain: bfloat16 [2048], replicated, may hold values from 0.099609375 to 1.8984375
- post_gain: bfloat16 [2048], replicated, may hold values from 0.099609375 to 1.8984375
- gate_proj: bfloat16 [8, 2048, 2048], P('sp', None, 'tp'), may hold values from -0.39648438 to 0.39648438
- up_proj: bfloat16 [8, 2048, 2048], P('sp', None, 'tp'), may hold values from -0.39648438 to 0.39648438
- down_proj: bfloat16 [8, 2048, 2048], P('sp', None, 'tp'), may hold values from -0.125 to 0.125
Outputs:
- layer_out: bfloat16 [2048, 2048], P(('sp', 'tp'))
Inputs may be any that keep to these rules, and one draw needn't show every extreme that they name: `route_ids`: in each aligned block of 64 positions, a row names 4 different experts and no expert is named by more than 64 rows; in every draw some expert reaches 64 in some block.
All inputs are finite; a program needn't handle non-finite values.
Results may differ from a plain program's by a relative error of at most 0.014.
Values may be sent and summed in bfloat16 or wider, within the bound.
A program may use at most 64 MiB of HBM per device.

v0:
```python
import jax
import jax.numpy as jnp
from jax import lax
from jax.sharding import PartitionSpec as P

clamp_limit = 7.0
sigmoid_scale = 1.702
epsilon = 1e-06


def passed_along(array, axis, by):
    count = lax.axis_size(axis)
    pairs = [(i, i + by) for i in range(count) if 0 <= i + by < count]
    return lax.ppermute(array, axis, pairs)


def clamped_units(gate_pre, up_pre):
    gate_cut = jnp.minimum(gate_pre, clamp_limit)
    up_cut = jnp.clip(up_pre, -clamp_limit, clamp_limit)
    return (up_cut + 1.0) * (gate_cut * jax.nn.sigmoid(sigmoid_scale * gate_cut))


def scaled_norm(values, gain):
    return (
        values
        * lax.rsqrt(jnp.mean(values * values, axis=-1, keepdims=True) + epsilon)
        * gain.astype(jnp.float32)
    )


def block_ranks(route_rows, experts, block_rows):
    flattened = route_rows.reshape(-1)
    entries = flattened.shape[0]
    span_width = block_rows * route_rows.shape[1]
    onehot = (flattened[:, None] == jnp.arange(experts, dtype=jnp.int32)[None, :]).astype(jnp.int32)
    blocked = onehot.reshape(entries // span_width, span_width, experts)
    before = jnp.cumsum(blocked, axis=1) - blocked
    return jnp.sum(before * blocked, axis=2).reshape(route_rows.shape)


def slot_picker(slot_index, table_size):
    matches = slot_index[None, :, :] == jnp.arange(table_size, dtype=jnp.int32)[:, None, None]
    return jnp.any(matches, axis=2).astype(jnp.bfloat16)


def local(
    stream_in,
    pre_gate,
    value_in,
    post_gate,
    conv_taps,
    out_weight,
    route_ids,
    route_weight,
    ffn_gain,
    post_gain,
    gate_proj,
    up_proj,
    down_proj,
):
    sp_count = lax.axis_size("sp")
    tp_count = lax.axis_size("tp")
    seq_rows = pre_gate.shape[0]
    own_rows = seq_rows // tp_count
    top_count = route_ids.shape[1]
    slots_each = 2 * own_rows * top_count // sp_count
    tap_count = conv_taps.shape[0]
    gated_input = (pre_gate.astype(jnp.float32) * value_in.astype(jnp.float32)).astype(jnp.bfloat16)
    rim_rows = passed_along(gated_input[seq_rows - tap_count + 1 :], "sp", 1)
    padded = jnp.concatenate([rim_rows, gated_input], 0).astype(jnp.float32)
    convolved = jnp.zeros(gated_input.shape, jnp.float32)
    for tap_index in range(tap_count):
        convolved = (
            convolved
            + conv_taps[tap_index].astype(jnp.float32)[None, :]
            * padded[tap_index : tap_index + seq_rows]
        )
    mixer_out = (post_gate.astype(jnp.float32) * convolved).astype(jnp.bfloat16)
    weight_rows = mixer_out
    projected = lax.psum_scatter(
        jnp.dot(weight_rows, out_weight, preferred_element_type=jnp.float32),
        "tp",
        scatter_dimension=0,
        tiled=True,
    )
    residual = (stream_in.astype(jnp.float32) + projected).astype(jnp.bfloat16)
    normed = scaled_norm(residual.astype(jnp.float32), ffn_gain).astype(jnp.bfloat16)
    slot_rank = block_ranks(route_ids, sp_count, own_rows)
    block_of = (jnp.arange(seq_rows, dtype=jnp.int32) // own_rows)[:, None]
    tp_index = lax.axis_index("tp")
    own_ids = lax.dynamic_slice_in_dim(route_ids, tp_index * own_rows, own_rows, 0)
    own_rank = lax.dynamic_slice_in_dim(slot_rank, tp_index * own_rows, own_rows, 0)
    own_slot = own_ids * slots_each + own_rank
    picker = slot_picker(own_slot, sp_count * slots_each)
    outgoing = jnp.dot(picker, normed, preferred_element_type=jnp.float32).astype(jnp.bfloat16)
    arrived = lax.all_to_all(outgoing, "sp", split_axis=0, concat_axis=0, tiled=True)
    portion = lax.all_gather(arrived, "tp", axis=0, tiled=True)
    gate_pre = jnp.dot(portion, gate_proj[0], preferred_element_type=jnp.float32)
    up_pre = jnp.dot(portion, up_proj[0], preferred_element_type=jnp.float32)
    hidden = clamped_units(gate_pre, up_pre).astype(jnp.bfloat16)
    weight_rows = down_proj[0]
    column_out = jnp.dot(
        lax.all_gather(hidden, "tp", axis=1, tiled=True),
        weight_rows,
        preferred_element_type=jnp.float32,
    ).astype(jnp.bfloat16)
    column_width = column_out.shape[1]
    returned = lax.all_to_all(
        column_out.reshape(tp_count, sp_count, slots_each, column_width),
        "sp",
        split_axis=1,
        concat_axis=1,
        tiled=True,
    )
    home_index = (block_of * sp_count + route_ids) * slots_each + slot_rank
    gathered_out = jnp.take(returned.reshape(-1, column_width), home_index.reshape(-1), axis=0)
    gathered_out = gathered_out.astype(jnp.float32).reshape(seq_rows, top_count, column_width)
    combined_cols = jnp.sum(gathered_out * route_weight[:, :, None], axis=1).astype(jnp.bfloat16)
    combined = lax.all_to_all(combined_cols, "tp", split_axis=0, concat_axis=1, tiled=True)
    layer_out = residual.astype(jnp.float32) + scaled_norm(combined.astype(jnp.float32), post_gain)
    return layer_out.astype(jnp.bfloat16)


def solution(mesh):
    placed = (
        P(("sp", "tp"), None),
        P("sp", "tp"),
        P("sp", "tp"),
        P("sp", "tp"),
        P(None, "tp"),
        P("tp", None),
        P("sp", None),
        P("sp", None),
        P(),
        P(),
        P("sp", None, "tp"),
        P("sp", None, "tp"),
        P("sp", None, "tp"),
    )
    return jax.shard_map(
        local, mesh=mesh, in_specs=placed, out_specs=P(("sp", "tp"), None), check_vma=False
    )
```

profile of v0, /device:TPU:0, one launch (start us, length us, event | category | flops | bytes accessed | tf_op | source)
XLA Modules:
  0.0 330.7 jit_solution(6274343751186609560)
XLA Ops:
  6.6 1.2 multiply_convert_fusion.1
  7.8 4.9 %collective-permute-start = (bf16[2,256]{1,0:T(2,128)(2,1)S(1)}, bf16[2,256]{1,0:T(2,128)(2,1)S(1)}, u32[]{:S(2)}, u32[]{:S(2)}) collective-permute-start(bf16[2,256]{1,0:T(2,128)(2,1)S(1)} %slice.38), channel_id=1, source_target_pairs={{0,4},{4,8},{8,12},{12,16},{16,20},{20,24},{24,28},{1,5},{5,9},{9,... | collective-permute-start | bytes 3080 | tf_op jit(solution)/shard_map/ppermute | solution.py:14
  12.6 0.8 slice_convert_fusion.2
  13.9 3.1 fusion.17
  17.6 2.3 reduce-window.6
  20.6 29.9 %reduce-scatter.2.cloned.1.call-done = f32[64,2048]{1,0:T(8,128)} async-done(((f32[256,2048]{1,0:T(8,128)}), f32[64,2048]{1,0:T(8,128)}) %reduce-scatter.2.cloned.1.call-update) | async-done | bytes 524304 | tf_op jit(solution)/shard_map/reduce_scatter | solution.py:80
  50.5 1.2 fusion.5
  51.7 0.8 convolution_convert_fusion.1
  52.5 53.5 %all_to_all.27 = bf16[8,64,2048]{2,1,0:T(8,128)(2,1)} all-to-all(bf16[8,64,2048]{2,1,0:T(8,128)(2,1)S(1)} %bitcast.40), channel_id=1, replica_groups=mesh['sp'=8,'tp'=4] {'sp'}, dimensions={0} | all-to-all | bytes 4194304 | tf_op jit(solution)/shard_map/all_to_all | solution.py:96
  106.1 56.5 %all-gather.3.cloned.1.call-done = bf16[2048,2048]{1,0:T(8,128)(2,1)} async-done(((bf16[512,2048]{1,0:T(8,128)(2,1)}), bf16[2048,2048]{1,0:T(8,128)(2,1)}) %all-gather.3.cloned.1.call-update) | async-done | bytes 8388624 | tf_op jit(solution)/shard_map/all_gather | solution.py:97
  162.5 7.7 %fusion.2 = f32[2048,512]{1,0:T(8,128)S(1)} fusion(bf16[2048,2048]{1,0:T(8,128)(2,1)} %all-gather.3.cloned.1.call-done, bf16[1,2048,512]{2,1,0:T(8,128)(2,1)S(1)} %copy-done), kind=kOutput, calls=%fused_computation.6 | convolution fusion | flops 4294967296 | bytes 14680064 | tf_op jit(solution)/shard_map/dot_general | solution.py:99
  170.2 6.7 %multiply_convert_fusion = bf16[2048,512]{1,0:T(8,128)(2,1)} fusion(f32[2048,512]{1,0:T(8,128)S(1)} %fusion.2, bf16[2048,2048]{1,0:T(8,128)(2,1)S(1)} %copy-done.6, bf16[1,2048,512]{2,1,0:T(8,128)(2,1)S(1)} %copy-done.7), kind=kOutput, calls=%fused_computation.1 | convolution fusion | flops 4305453056 | bytes 16777216 | tf_op jit(solution)/shard_map/dot_general | solution.py:98
  177.0 58.4 %all-gather.5.cloned.1.call-done = bf16[2048,2048]{1,0:T(8,128)(2,1)} async-done(((bf16[2048,512]{1,0:T(8,128)(2,1)}), bf16[2048,2048]{1,0:T(8,128)(2,1)}) %all-gather.5.cloned.1.call-update) | async-done | bytes 8388624 | tf_op jit(solution)/shard_map/all_gather | solution.py:103
  235.4 8.5 %convolution_convert_fusion = bf16[2048,512]{1,0:T(8,128)(2,1)S(1)} fusion(bf16[2048,2048]{1,0:T(8,128)(2,1)} %all-gather.5.cloned.1.call-done, bf16[1,2048,512]{2,1,0:T(8,128)(2,1)} %param.25), kind=kOutput, calls=%fused_computation.2 | convolution fusion | flops 4296015872 | bytes 12582912 | tf_op jit(solution)/shard_map/dot_general | solution.py:102
  243.9 1.4 copy.61
  245.3 5.5 %all-to-all-start.1 = ((bf16[4,8,64,512]{3,2,0,1:T(8,128)(2,1)}), bf16[4,8,64,512]{3,2,0,1:T(8,128)(2,1)}, u32[]{:S(2)}, u32[]{:S(2)}) async-start(bf16[4,8,64,512]{3,2,0,1:T(8,128)(2,1)} %copy.61), calls=%async_computation.2 | async-start | bytes 4194304 | tf_op jit(solution)/shard_map/all_to_all | solution.py:108
  252.1 47.5 %all-to-all-done.1 = bf16[4,8,64,512]{3,2,0,1:T(8,128)(2,1)} async-done(((bf16[4,8,64,512]{3,2,0,1:T(8,128)(2,1)}), bf16[4,8,64,512]{3,2,0,1:T(8,128)(2,1)}, u32[]{:S(2)}, u32[]{:S(2)}) %all-to-all-start.1) | async-done | bytes 2097184 | tf_op jit(solution)/shard_map/all_to_all | solution.py:108
  299.6 3.1 copy.62
  302.7 5.9 %gather_fusion = bf16[1024,512]{1,0:T(8,128)(2,1)S(1)} fusion(bf16[2048,512]{1,0:T(8,128)(2,1)} %bitcast.38, s32[1024]{0:T(1024)S(1)} %broadcast_clamp_fusion), kind=kCustom, calls=%fused_computation | custom fusion | bytes 2101248 | tf_op jit(solution)/shard_map/jit(_take)/gather | solution.py:116
  308.6 1.1 gather.7
  309.7 4.0 %multiply_reduce_fusion = bf16[256,512]{1,0:T(8,128)(2,1)} fusion(f32[256,4]{1,0:T(8,128)S(1)} %copy.64, bf16[256,4,512]{2,1,0:T(4,128)(2,1)} %gather.7, pred[256,4]{1,0:T(8,128)(4,1)} %copy.59), kind=kLoop, calls=%fused_computation.8 | loop fusion | flops 1966080 | bytes 1315840 | tf_op jit(solution)/shard_map/reduce_sum | solution.py:118
  313.7 3.4 %all-to-all-start.2 = ((bf16[4,64,512]{2,1,0:T(8,128)(2,1)}), bf16[4,64,512]{2,1,0:T(8,128)(2,1)S(1)}, u32[]{:S(2)}, u32[]{:S(2)}) async-start(bf16[4,64,512]{2,1,0:T(8,128)(2,1)} %bitcast.14), calls=%async_computation.3 | async-start | bytes 524288 | tf_op jit(solution)/shard_map/all_to_all | solution.py:119
  317.1 6.0 %all-to-all-done.2 = bf16[4,64,512]{2,1,0:T(8,128)(2,1)S(1)} async-done(((bf16[4,64,512]{2,1,0:T(8,128)(2,1)}), bf16[4,64,512]{2,1,0:T(8,128)(2,1)S(1)}, u32[]{:S(2)}, u32[]{:S(2)}) %all-to-all-start.2) | async-done | bytes 262176 | tf_op jit(solution)/shard_map/all_to_all | solution.py:119
  323.3 0.9 fusion.8
  (54 shorter events, 3.3 us)
Async XLA Ops:
  6.5 156.0 %copy-start = (bf16[1,2048,512]{2,1,0:T(8,128)(2,1)S(1)}, bf16[1,2048,512]{2,1,0:T(8,128)(2,1)}, u32[]{:S(2)}) copy-start(bf16[1,2048,512]{2,1,0:T(8,128)(2,1)} %param.24) | copy-start | bytes 6291460
  6.5 10.6 %copy-start.2 = (s32[256,4]{0,1:T(4,128)S(1)}, s32[256,4]{0,1:T(4,128)}, u32[]{:S(2)}) copy-start(s32[256,4]{0,1:T(4,128)} %param.19) | copy-start | bytes 12292
  6.5 13.8 %copy-start.3 = (bf16[2048]{0:T(1024)(128)(2,1)S(1)}, bf16[2048]{0:T(1024)(128)(2,1)}, u32[]{:S(2)}) copy-start(bf16[2048]{0:T(1024)(128)(2,1)} %param.21) | copy-start | bytes 12292
  6.5 43.9 %copy-start.1 = (bf16[64,2048]{1,0:T(8,128)(2,1)S(1)}, bf16[64,2048]{1,0:T(8,128)(2,1)}, u32[]{:S(2)}) copy-start(bf16[64,2048]{1,0:T(8,128)(2,1)} %param.13) | copy-start | bytes 786436
  6.5 43.9 %reduce-scatter.2.cloned.1.call-start = ((), (), s32[]{:S(2)}) async-start(), calls=%async_computation.4 | async-start | bytes 2621440 | tf_op jit(solution)/shard_map/reduce_scatter | solution.py:80
  7.8 6.2 %collective-permute-start = (bf16[2,256]{1,0:T(2,128)(2,1)S(1)}, bf16[2,256]{1,0:T(2,128)(2,1)S(1)}, u32[]{:S(2)}, u32[]{:S(2)}) collective-permute-start(bf16[2,256]{1,0:T(2,128)(2,1)S(1)} %slice.38), channel_id=1, source_target_pairs={{0,4},{4,8},{8,12},{12,16},{16,20},{20,24},{24,28},{1,5},{5,9},{9,... | collective-permute-start | bytes 3080 | tf_op jit(solution)/shard_map/ppermute | solution.py:14
  17.1 145.4 %all-gather.3.cloned.1.call-start = ((), (), s32[]{:S(2)}) async-start(), calls=%async_computation.5 | async-start | bytes 10485760 | tf_op jit(solution)/shard_map/all_gather | solution.py:97
  106.0 129.3 %all-gather.5.cloned.1.call-start = ((), (), s32[]{:S(2)}) async-start(), calls=%async_computation.6 | async-start | bytes 10485760 | tf_op jit(solution)/shard_map/all_gather | solution.py:103
  162.5 7.7 %copy-start.6 = (bf16[2048,2048]{1,0:T(8,128)(2,1)S(1)}, bf16[2048,2048]{1,0:T(8,128)(2,1)}, u32[]{:S(2)}) copy-start(bf16[2048,2048]{1,0:T(8,128)(2,1)} %all-gather.3.cloned.1.call-done) | copy-start | bytes 25165828
  162.5 7.7 %copy-start.7 = (bf16[1,2048,512]{2,1,0:T(8,128)(2,1)S(1)}, bf16[1,2048,512]{2,1,0:T(8,128)(2,1)}, u32[]{:S(2)}) copy-start(bf16[1,2048,512]{2,1,0:T(8,128)(2,1)} %param.23) | copy-start | bytes 6291460
  243.9 8.0 %copy-start.4 = (f32[256,4]{0,1:T(4,128)S(1)}, f32[256,4]{0,1:T(4,128)}, u32[]{:S(2)}) copy-start(f32[256,4]{0,1:T(4,128)} %param.20) | copy-start | bytes 12292
  245.3 54.3 %all-to-all-start.1 = ((bf16[4,8,64,512]{3,2,0,1:T(8,128)(2,1)}), bf16[4,8,64,512]{3,2,0,1:T(8,128)(2,1)}, u32[]{:S(2)}, u32[]{:S(2)}) async-start(bf16[4,8,64,512]{3,2,0,1:T(8,128)(2,1)} %copy.61), calls=%async_computation.2 | async-start | bytes 4194304 | tf_op jit(solution)/shard_map/all_to_all | solution.py:108
  302.7 14.4 %copy-start.5 = (bf16[2048]{0:T(1024)(128)(2,1)S(1)}, bf16[2048]{0:T(1024)(128)(2,1)}, u32[]{:S(2)}) copy-start(bf16[2048]{0:T(1024)(128)(2,1)} %param.22) | copy-start | bytes 12292
  313.7 9.4 %all-to-all-start.2 = ((bf16[4,64,512]{2,1,0:T(8,128)(2,1)}), bf16[4,64,512]{2,1,0:T(8,128)(2,1)S(1)}, u32[]{:S(2)}, u32[]{:S(2)}) async-start(bf16[4,64,512]{2,1,0:T(8,128)(2,1)} %bitcast.14), calls=%async_computation.3 | async-start | bytes 524288 | tf_op jit(solution)/shard_map/all_to_all | solution.py:119
Sparse Core Ops, SparseCore 0:
  17.2 33.2 reduce-scatter.1
  106.1 56.3 all-gather.2
  177.1 58.2 all-gather.4
where the time goes:
time: 331 us
  waiting for transfers between devices  199 us (60%)
  blocking collectives  53.5 us (16%)
  matrix products  26.8 us (8%)
  starting transfers between devices  13.9 us (4%)
  local copies, waits for them, and re-layouts  13.6 us (4%)
  between operations  13.3 us (4%)
  other arithmetic  10.9 us (3%)
    all_gather x1, waiting for transfers between devices, local(): lax.all_gather(hidden, 'tp', axis=1, tiled=True)  58.4 us
    all_gather x1, waiting for transfers between devices, local(): portion = lax.all_gather(arrived, 'tp', axis=0, tiled=True)  56.5 us
    all_to_all x1, blocking collectives, local(): lax.all_to_all(outgoing, 'sp', split_axis=0, concat_axis=0, tiled=True)  53.5 us
    all_to_all x1, waiting for transfers between devices, local(): lax.all_to_all(column_out.reshape(tp_count, sp_count, slots_each, column_...  47.5 us
    reduce_scatter x1, waiting for transfers between devices, local(): lax.psum_scatter(jnp.dot(weight_rows, out_weight, preferred_element_type=...  29.9 us
    dot_general x1, matrix products, local(): jnp.dot(lax.all_gather(hidden, 'tp', axis=1, tiled=True), weight_rows, pr...  8.49 us
    dot_general x1, matrix products, local(): up_pre = jnp.dot(portion, up_proj[0], preferred_element_type=jnp.float32)  7.66 us
    gather x2, local copies, waits for them, and re-layouts, local(): jnp.take(returned.reshape(-1, column_width), home_index.reshape(-1), axis=0)  6.98 us
  transfers between devices with their start and end apart: 6, of which 6 were waited for; matrix products, arithmetic and copies ran while one was open for 2% of the time, Pallas kernels for 0%

commit v1 on v0

--- a/solution.py
+++ b/solution.py
@@ -94,7 +94,12 @@
     picker = slot_picker(own_slot, sp_count * slots_each)
     outgoing = jnp.dot(picker, normed, preferred_element_type=jnp.float32).astype(jnp.bfloat16)
     arrived = lax.all_to_all(outgoing, "sp", split_axis=0, concat_axis=0, tiled=True)
-    portion = lax.all_gather(arrived, "tp", axis=0, tiled=True)
+    ring = [arrived]
+    for hop in range(3):
+        ring.append(lax.ppermute(ring[-1], "tp", [(dev, (dev + 1) % 4) for dev in range(4)]))
+    portion = jnp.roll(
+        jnp.concatenate(ring[::-1], axis=0), (lax.axis_index("tp") + 1) * ring[0].shape[0], axis=0
+    )
     gate_pre = jnp.dot(portion, gate_proj[0], preferred_element_type=jnp.float32)
     up_pre = jnp.dot(portion, up_proj[0], preferred_element_type=jnp.float32)
     hidden = clamped_units(gate_pre, up_pre).astype(jnp.bfloat16)

time: 331 us -> 358 us (1.082)
  waiting for transfers between devices: 199 us -> 217 us
  local copies, waits for them, and re-layouts: 13.6 us -> 24.3 us
    ppermute x0 -> x3, waiting for transfers between devices: none -> 76.8 us  [local(): lax.ppermute(ring[-1], 'tp', [(dev, (dev + 1) % 4) for dev in range(4)])]
    all_gather x1 -> x0, waiting for transfers between devices: 56.5 us -> none  [local(): portion = lax.all_gather(arrived, 'tp', axis=0, tiled=True)]
    unnamed x18 -> x31, local copies, waits for them, and re-layouts: 0.3 us -> 10.9 us
  transfers between devices with their start and end apart: 6 -> 8, of which waited for: 6 -> 8; matrix products, arithmetic and copies ran while one was open for 2% -> 2% of each run, Pallas kernels for 0% -> 0%
where the time goes in v1:
time: 358 us; the launch traced here: 357 us
  waiting for transfers between devices  217 us (61%)
  blocking collectives  53.4 us (15%)
  local copies, waits for them, and re-layouts  24.3 us (7%)
  matrix products  23.6 us (7%)
  starting transfers between devices  13.9 us (4%)
  between operations  13.7 us (4%)
  other arithmetic  10.9 us (3%)
    ppermute x3, waiting for transfers between devices, local(): lax.ppermute(ring[-1], 'tp', [(dev, (dev + 1) % 4) for dev in range(4)])  76.8 us
    all_gather x1, waiting for transfers between devices, local(): lax.all_gather(hidden, 'tp', axis=1, tiled=True)  56.5 us
    all_to_all x1, blocking collectives, local(): lax.all_to_all(outgoing, 'sp', split_axis=0, concat_axis=0, tiled=True)  53.4 us
    all_to_all x1, waiting for transfers between devices, local(): lax.all_to_all(column_out.reshape(tp_count, sp_count, slots_each, column_...  47.5 us
    reduce_scatter x1, waiting for transfers between devices, local(): lax.psum_scatter(jnp.dot(weight_rows, out_weight, preferred_element_type=...  29.8 us
    unnamed x31, local copies, waits for them, and re-layouts  10.9 us
    dot_general x1, matrix products, local(): jnp.dot(lax.all_gather(hidden, 'tp', axis=1, tiled=True), weight_rows, pr...  8.49 us
  transfers between devices with their start and end apart: 8, of which 8 were waited for; matrix products, arithmetic and copies ran while one was open for 2% of the time, Pallas kernels for 0%

profile of v1, /device:TPU:0, one launch (start us, length us, event | category | flops | bytes accessed | tf_op | source)
XLA Modules:
  0.0 356.9 jit_solution(15303656589087495576)
XLA Ops:
  7.8 4.9 %collective-permute-start = (bf16[2,256]{1,0:T(2,128)(2,1)S(1)}, bf16[2,256]{1,0:T(2,128)(2,1)S(1)}, u32[]{:S(2)}, u32[]{:S(2)}) collective-permute-start(bf16[2,256]{1,0:T(2,128)(2,1)S(1)} %slice.38), channel_id=1, source_target_pairs={{0,4},{4,8},{8,12},{12,16},{16,20},{20,24},{24,28},{1,5},{5,9},{9,... | collective-permute-start | bytes 3080 | tf_op jit(solution)/shard_map/ppermute | solution.py:14
  13.9 3.1 fusion.22
  17.6 2.3 reduce-window.6
  20.6 29.8 %reduce-scatter.2.cloned.1.call-done = f32[64,2048]{1,0:T(8,128)} async-done(((f32[256,2048]{1,0:T(8,128)}), f32[64,2048]{1,0:T(8,128)}) %reduce-scatter.2.cloned.1.call-update) | async-done | bytes 524304 | tf_op jit(solution)/shard_map/reduce_scatter | solution.py:80
  52.5 53.4 %all_to_all.27 = bf16[8,64,2048]{2,1,0:T(8,128)(2,1)S(1)} all-to-all(bf16[8,64,2048]{2,1,0:T(8,128)(2,1)S(1)} %bitcast.40), channel_id=1, replica_groups=mesh['sp'=8,'tp'=4] {'sp'}, dimensions={0} | all-to-all | bytes 4194304 | tf_op jit(solution)/shard_map/all_to_all | solution.py:96
  107.2 25.5 %collective-permute-done.1 = bf16[512,2048]{1,0:T(8,128)(2,1)S(1)} collective-permute-done((bf16[512,2048]{1,0:T(8,128)(2,1)S(1)}, bf16[512,2048]{1,0:T(8,128)(2,1)S(1)}, u32[]{:S(2)}, u32[]{:S(2)}) %collective-permute-start.1) | collective-permute-done | bytes 2097184 | tf_op jit(solution)/shard_map/ppermute | solution.py:99
  134.0 25.6 %collective-permute-done.2 = bf16[512,2048]{1,0:T(8,128)(2,1)} collective-permute-done((bf16[512,2048]{1,0:T(8,128)(2,1)S(1)}, bf16[512,2048]{1,0:T(8,128)(2,1)}, u32[]{:S(2)}, u32[]{:S(2)}) %collective-permute-start.2) | collective-permute-done | bytes 2097184 | tf_op jit(solution)/shard_map/ppermute | solution.py:99
  159.6 25.8 %collective-permute-done.3 = bf16[512,2048]{1,0:T(8,128)(2,1)} collective-permute-done((bf16[512,2048]{1,0:T(8,128)(2,1)}, bf16[512,2048]{1,0:T(8,128)(2,1)}, u32[]{:S(2)}, u32[]{:S(2)}) %collective-permute-start.3) | collective-permute-done | bytes 2097184 | tf_op jit(solution)/shard_map/ppermute | solution.py:99
  185.3 1.8 constant_dynamic-update-slice_fusion.7
  187.2 2.0 constant_dynamic-update-slice_fusion.6
  189.5 1.8 constant_dynamic-update-slice_fusion.3
  191.4 1.8 constant_dynamic-update-slice_fusion.2
  193.5 4.5 %fusion.2 = f32[2048,512]{1,0:T(8,128)S(1)} fusion(bf16[4096,2048]{1,0:T(8,128)(2,1)S(1)} %constant_dynamic-update-slice_fusion, s32[]{:T(128)S(6)} %select_n.52, bf16[1,2048,512]{2,1,0:T(8,128)(2,1)S(1)} %copy-done), kind=kOutput, calls=%fused_computation.3 | convolution fusion | flops 4294967296 | bytes 14680068 | tf_op jit(solution)/shard_map/dot_general | solution.py:104
  198.1 6.7 %multiply_convert_fusion = bf16[2048,512]{1,0:T(8,128)(2,1)} fusion(f32[2048,512]{1,0:T(8,128)S(1)} %fusion.2, bf16[4096,2048]{1,0:T(8,128)(2,1)S(1)} %constant_dynamic-update-slice_fusion, s32[]{:T(128)S(6)} %select_n.52, bf16[1,2048,512]{2,1,0:T(8,128)(2,1)S(1)} %copy-done.10), kind=kOutput, calls=%fused_computation.5 | convolution fusion | flops 4305453056 | bytes 16777220 | tf_op jit(solution)/shard_map/dot_general | solution.py:103
  204.7 56.5 %all-gather.2.cloned.1.call-done = bf16[2048,2048]{1,0:T(8,128)(2,1)} async-done(((bf16[2048,512]{1,0:T(8,128)(2,1)}), bf16[2048,2048]{1,0:T(8,128)(2,1)}) %all-gather.2.cloned.1.call-update) | async-done | bytes 8388624 | tf_op jit(solution)/shard_map/all_gather | solution.py:108
  261.3 8.5 %convolution_convert_fusion = bf16[2048,512]{1,0:T(8,128)(2,1)S(1)} fusion(bf16[2048,2048]{1,0:T(8,128)(2,1)} %all-gather.2.cloned.1.call-done, bf16[1,2048,512]{2,1,0:T(8,128)(2,1)} %param.25), kind=kOutput, calls=%fused_computation.6 | convolution fusion | flops 4296015872 | bytes 12582912 | tf_op jit(solution)/shard_map/dot_general | solution.py:107
  269.8 1.4 copy.61
  271.2 5.5 %all-to-all-start.1 = ((bf16[4,8,64,512]{3,2,0,1:T(8,128)(2,1)}), bf16[4,8,64,512]{3,2,0,1:T(8,128)(2,1)}, u32[]{:S(2)}, u32[]{:S(2)}) async-start(bf16[4,8,64,512]{3,2,0,1:T(8,128)(2,1)} %copy.61), calls=%async_computation.2 | async-start | bytes 4194304 | tf_op jit(solution)/shard_map/all_to_all | solution.py:113
  278.0 47.5 %all-to-all-done.1 = bf16[4,8,64,512]{3,2,0,1:T(8,128)(2,1)} async-done(((bf16[4,8,64,512]{3,2,0,1:T(8,128)(2,1)}), bf16[4,8,64,512]{3,2,0,1:T(8,128)(2,1)}, u32[]{:S(2)}, u32[]{:S(2)}) %all-to-all-start.1) | async-done | bytes 2097184 | tf_op jit(solution)/shard_map/all_to_all | solution.py:113
  325.5 3.1 copy.62
  328.6 5.9 %gather_fusion = bf16[1024,512]{1,0:T(8,128)(2,1)S(1)} fusion(bf16[2048,512]{1,0:T(8,128)(2,1)} %bitcast.36, s32[1024]{0:T(1024)S(1)} %broadcast_clamp_fusion), kind=kCustom, calls=%fused_computation | custom fusion | bytes 2101248 | tf_op jit(solution)/shard_map/jit(_take)/gather | solution.py:121
  335.6 4.0 %multiply_reduce_fusion = bf16[256,512]{1,0:T(8,128)(2,1)} fusion(f32[256,4]{1,0:T(8,128)S(1)} %copy.64, bf16[256,4,512]{2,1,0:T(4,128)(2,1)} %gather.7, pred[256,4]{1,0:T(8,128)(4,1)} %copy.59), kind=kLoop, calls=%fused_computation.11 | loop fusion | flops 1966080 | bytes 1315840 | tf_op jit(solution)/shard_map/reduce_sum | solution.py:123
  339.6 3.4 all-to-all-start.2
  343.0 6.0 %all-to-all-done.2 = bf16[4,64,512]{2,1,0:T(8,128)(2,1)S(1)} async-done(((bf16[4,64,512]{2,1,0:T(8,128)(2,1)}), bf16[4,64,512]{2,1,0:T(8,128)(2,1)S(1)}, u32[]{:S(2)}, u32[]{:S(2)}) %all-to-all-start.2) | async-done | bytes 262176 | tf_op jit(solution)/shard_map/all_to_all | solution.py:124
  (71 shorter events, 12.5 us)
Async XLA Ops:
  6.5 187.0 %copy-start = (bf16[1,2048,512]{2,1,0:T(8,128)(2,1)S(1)}, bf16[1,2048,512]{2,1,0:T(8,128)(2,1)}, u32[]{:S(2)}) copy-start(bf16[1,2048,512]{2,1,0:T(8,128)(2,1)} %param.24) | copy-start | bytes 6291460
  6.5 10.6 %copy-start.6 = (s32[256,4]{0,1:T(4,128)S(1)}, s32[256,4]{0,1:T(4,128)}, u32[]{:S(2)}) copy-start(s32[256,4]{0,1:T(4,128)} %param.19) | copy-start | bytes 12292
  6.5 13.8 %copy-start.7 = (bf16[2048]{0:T(1024)(128)(2,1)S(1)}, bf16[2048]{0:T(1024)(128)(2,1)}, u32[]{:S(2)}) copy-start(bf16[2048]{0:T(1024)(128)(2,1)} %param.21) | copy-start | bytes 12292
  6.5 43.9 %copy-start.5 = (bf16[64,2048]{1,0:T(8,128)(2,1)S(1)}, bf16[64,2048]{1,0:T(8,128)(2,1)}, u32[]{:S(2)}) copy-start(bf16[64,2048]{1,0:T(8,128)(2,1)} %param.13) | copy-start | bytes 786436
  6.5 43.9 %reduce-scatter.2.cloned.1.call-start = ((), (), s32[]{:S(2)}) async-start(), calls=%async_computation.4 | async-start | bytes 2621440 | tf_op jit(solution)/shard_map/reduce_scatter | solution.py:80
  7.8 6.2 %collective-permute-start = (bf16[2,256]{1,0:T(2,128)(2,1)S(1)}, bf16[2,256]{1,0:T(2,128)(2,1)S(1)}, u32[]{:S(2)}, u32[]{:S(2)}) collective-permute-start(bf16[2,256]{1,0:T(2,128)(2,1)S(1)} %slice.38), channel_id=1, source_target_pairs={{0,4},{4,8},{8,12},{12,16},{16,20},{20,24},{24,28},{1,5},{5,9},{9,... | collective-permute-start | bytes 3080 | tf_op jit(solution)/shard_map/ppermute | solution.py:14
  17.1 244.2 %all-gather.2.cloned.1.call-start = ((), (), s32[]{:S(2)}) async-start(), calls=%async_computation.5 | async-start | bytes 10485760 | tf_op jit(solution)/shard_map/all_gather | solution.py:108
  105.9 1.3 copy-start.1
  107.2 25.5 %collective-permute-start.1 = (bf16[512,2048]{1,0:T(8,128)(2,1)S(1)}, bf16[512,2048]{1,0:T(8,128)(2,1)S(1)}, u32[]{:S(2)}, u32[]{:S(2)}) collective-permute-start(bf16[512,2048]{1,0:T(8,128)(2,1)S(1)} %bitcast.37), channel_id=1, source_target_pairs={{0,1},{1,2},{2,3},{3,0},{4,5},{5,6},{6,7},{7,4},{8,9},{9,10},{10,1... | collective-permute-start | bytes 6291464 | tf_op jit(solution)/shard_map/ppermute | solution.py:99
  132.7 1.3 copy-start.3
  134.0 25.6 %collective-permute-start.2 = (bf16[512,2048]{1,0:T(8,128)(2,1)S(1)}, bf16[512,2048]{1,0:T(8,128)(2,1)}, u32[]{:S(2)}, u32[]{:S(2)}) collective-permute-start(bf16[512,2048]{1,0:T(8,128)(2,1)S(1)} %collective-permute-done.1), channel_id=1, source_target_pairs={{0,1},{1,2},{2,3},{3,0},{4,5},{5,6},{6,7},{7,4},{8,9},{9,10},{10,1... | collective-permute-start | bytes 6291464 | tf_op jit(solution)/shard_map/ppermute | solution.py:99
  159.6 25.8 %collective-permute-start.3 = (bf16[512,2048]{1,0:T(8,128)(2,1)}, bf16[512,2048]{1,0:T(8,128)(2,1)}, u32[]{:S(2)}, u32[]{:S(2)}) collective-permute-start(bf16[512,2048]{1,0:T(8,128)(2,1)} %collective-permute-done.2), channel_id=1, source_target_pairs={{0,1},{1,2},{2,3},{3,0},{4,5},{5,6},{6,7},{7,4},{8,9},{9,10},{10,1... | collective-permute-start | bytes 6291464 | tf_op jit(solution)/shard_map/ppermute | solution.py:99
  159.6 29.6 %copy-start.4 = (bf16[512,2048]{1,0:T(8,128)(2,1)S(1)}, bf16[512,2048]{1,0:T(8,128)(2,1)}, u32[]{:S(2)}) copy-start(bf16[512,2048]{1,0:T(8,128)(2,1)} %copy-done.3) | copy-start | bytes 6291460
  187.2 2.2 copy-start.2
  193.5 4.5 %copy-start.10 = (bf16[1,2048,512]{2,1,0:T(8,128)(2,1)S(1)}, bf16[1,2048,512]{2,1,0:T(8,128)(2,1)}, u32[]{:S(2)}) copy-start(bf16[1,2048,512]{2,1,0:T(8,128)(2,1)} %param.23) | copy-start | bytes 6291460
  269.8 8.0 %copy-start.8 = (f32[256,4]{0,1:T(4,128)S(1)}, f32[256,4]{0,1:T(4,128)}, u32[]{:S(2)}) copy-start(f32[256,4]{0,1:T(4,128)} %param.20) | copy-start | bytes 12292
  271.2 54.3 %all-to-all-start.1 = ((bf16[4,8,64,512]{3,2,0,1:T(8,128)(2,1)}), bf16[4,8,64,512]{3,2,0,1:T(8,128)(2,1)}, u32[]{:S(2)}, u32[]{:S(2)}) async-start(bf16[4,8,64,512]{3,2,0,1:T(8,128)(2,1)} %copy.61), calls=%async_computation.2 | async-start | bytes 4194304 | tf_op jit(solution)/shard_map/all_to_all | solution.py:113
  328.6 14.4 %copy-start.9 = (bf16[2048]{0:T(1024)(128)(2,1)S(1)}, bf16[2048]{0:T(1024)(128)(2,1)}, u32[]{:S(2)}) copy-start(bf16[2048]{0:T(1024)(128)(2,1)} %param.22) | copy-start | bytes 12292
  339.6 9.4 %all-to-all-start.2 = ((bf16[4,64,512]{2,1,0:T(8,128)(2,1)}), bf16[4,64,512]{2,1,0:T(8,128)(2,1)S(1)}, u32[]{:S(2)}, u32[]{:S(2)}) async-start(bf16[4,64,512]{2,1,0:T(8,128)(2,1)} %bitcast.14), calls=%async_computation.3 | async-start | bytes 524288 | tf_op jit(solution)/shard_map/all_to_all | solution.py:124
Sparse Core Ops, SparseCore 0:
  17.2 33.2 reduce-scatter.1
  204.9 56.3 all-gather.1
